TPU v7x, 32 devices: a whole 2x2x4 slice. The times are simulated.
32 devices in a mesh: sp: 8 (over z, x), tp: 4 (over y, core).
Axes of the slice: x: 2, y: 2, z: 4, core: 2. Of those that a mesh axis runs over, the one named last changes fastest.
Arguments:
- residual_in: bfloat16 [2048, 2048], P(('sp', 'tp')), may hold values from -6 to 6
- queries: bfloat16 [2048, 512], P('sp', 'tp'), may hold values from -6 to 6
- key_rows: bfloat16 [2048, 512], P('sp', 'tp'), may hold values from -6 to 6
- value_rows: bfloat16 [2048, 1024], P('sp', 'tp'), may hold values from -6 to 6
- out_gate: bfloat16 [2048, 1024], P('sp', 'tp'), may hold values from -6 to 6
- decay_logit: float32 [2048, 512], P('sp', 'tp'), may hold values from -30 to 30
- head_gain: bfloat16 [128], replicated, may hold values from 0.099609375 to 1.8984375
- w_out: bfloat16 [1024, 2048], replicated, may hold values from -0.1875 to 0.1875
- ffn_gain: bfloat16 [2048], replicated, may hold values from 0.099609375 to 1.8984375
- routing: int32 [2048, 4], P('sp'), may hold values from 0 to 7, all different within a row; in each aligned block of 64 rows (0 to 63, 64 to 127, ...) at most 64 rows name the same one
- route_weight: float32 [2048, 4], P(('sp', 'tp')), may hold values from 0.05 to 0.6
- w_gate: bfloat16 [8, 2048, 2048], P('sp', None, 'tp'), may hold values from -4 to 4
- w_up: bfloat16 [8, 2048, 2048], P('sp', None, 'tp'), may hold values from -4 to 4
- w_down: bfloat16 [8, 2048, 2048], P('sp', 'tp'), may hold values from -0.125 to 0.125
Outputs:
- layer_out: bfloat16 [2048, 2048], P(('sp', 'tp'))
Inputs may be any that keep to these rules, and one draw needn't show every extreme that they name: `routing`: each row names 4 different experts. In each aligned block of 64 rows no expert is named more than 64 times, a bound that some blocks reach.
All inputs are finite; a program needn't handle non-finite values.
Results may differ from a plain program's by a relative error of at most 0.03.
Values may be sent and summed in bfloat16 or wider, within the bound.
A program may use at most 128 MiB of HBM per device.

v0:
```python
import jax
import jax.numpy as jnp
from jax import lax
from jax.sharding import PartitionSpec as P

DK = 64
DV = 128
BLOCK = 64


DECAY_TEMP = 16.0
CLAMP_LIMIT = 7.0
SIGMOID_SLOPE = 1.702
NORM_EPS = 1e-06
EXACT_PRECISION = lax.Precision.HIGHEST


def entering(value, axis, combine, identity):
    size, place = (lax.axis_size(axis), lax.axis_index(axis))
    everything = jax.tree.map(
        lambda part, kind: lax.all_gather(part.astype(kind), axis),
        value,
        (jnp.bfloat16, jnp.bfloat16),
    )
    start = jax.tree.map(
        lambda part, zero: jnp.broadcast_to(jnp.asarray(zero, part.dtype), part.shape),
        value,
        identity,
    )

    def turn(k, before):
        reached = k < place
        new = combine(
            before, jax.tree.map(lambda part, own: part[k].astype(own.dtype), everything, value)
        )
        return jax.tree.map(lambda a, b: jnp.where(reached, a, b), new, before)

    return lax.fori_loop(0, size, turn, start)


def block_parts(query_blk, key_blk, value_blk, logdecay_blk):
    cumulative = jnp.cumsum(logdecay_blk, axis=2)
    length = cumulative.shape[2]
    causal = (jnp.arange(length)[:, None] >= jnp.arange(length)[None, :])[:, :, None]
    spread = cumulative[:, :, :, None, :] - cumulative[:, :, None, :, :]
    weighted = query_blk[:, :, :, None, :] * jnp.exp(jnp.where(causal, spread, -jnp.inf))
    scores = jnp.einsum("nhtsk,nhsk->nhts", weighted, key_blk, precision=EXACT_PRECISION)
    inner_part = jnp.einsum("nhts,nhsv->nhtv", scores, value_blk, precision=EXACT_PRECISION)
    ending = cumulative[:, :, -1:, :]
    contrib = jnp.einsum(
        "nhsk,nhsv->nhkv",
        key_blk * jnp.exp(ending - cumulative),
        value_blk,
        precision=EXACT_PRECISION,
    )
    return (inner_part, query_blk * jnp.exp(cumulative), contrib, jnp.exp(ending[:, :, 0, :]))


def carry_blocks(query_dec, contrib, passing, begin):

    def advance(recurrent_state, inputs):
        current_query, contrib_now, passing_now = inputs
        state_readout = jnp.einsum(
            "uaz,uze->uae", current_query, recurrent_state, precision=EXACT_PRECISION
        )
        return (passing_now[..., None] * recurrent_state + contrib_now, state_readout)

    final_state, readouts = lax.scan(advance, begin, (query_dec, contrib, passing))
    return (readouts, final_state)


def fold_state(contrib, passing):

    def absorb(recurrent_state, inputs):
        contrib_now, passing_now = inputs
        return (passing_now[..., None] * recurrent_state + contrib_now, None)

    final_state, _ = lax.scan(absorb, jnp.zeros_like(contrib[0]), (contrib, passing))
    return final_state


def combine_states(earlier, following):
    return (earlier[0] * following[0], following[0][..., None] * earlier[1] + following[1])


def carried_state(total_decay, local_state):
    identity = (jnp.ones_like(total_decay), jnp.zeros_like(local_state))
    return entering((total_decay, local_state), "sp", combine_states, identity)[1]


def to_blocks(array, head_width):
    tokens = array.shape[0]
    head_count = array.shape[1] // head_width
    return (
        array.astype(jnp.float32)
        .reshape(tokens // BLOCK, BLOCK, head_count, head_width)
        .transpose(0, 2, 1, 3)
    )


def finish_heads(blocks_out, head_gain, out_gate):
    count_blk, head_count, length, head_width = blocks_out.shape
    tokens = count_blk * length
    attended = blocks_out.transpose(0, 2, 1, 3).reshape(tokens, head_count, head_width)
    inv_scale = lax.rsqrt(jnp.mean(attended * attended, axis=-1, keepdims=True) + NORM_EPS)
    headed = attended * inv_scale * head_gain.astype(jnp.float32)
    gated = headed.reshape(tokens, head_count * head_width) * jax.nn.silu(
        out_gate.astype(jnp.float32)
    )
    return gated.astype(jnp.bfloat16)


def norm_rows(residual, gain_vec):
    values = residual.astype(jnp.float32)
    inv_scale = lax.rsqrt(jnp.mean(values * values, axis=-1, keepdims=True) + NORM_EPS)
    return (values * inv_scale * gain_vec.astype(jnp.float32)).astype(jnp.bfloat16)


def clamped_unit(gate_pre, up_pre):
    gate_cut = jnp.minimum(gate_pre, CLAMP_LIMIT)
    up_cut = jnp.clip(up_pre, -CLAMP_LIMIT, CLAMP_LIMIT)
    return (up_cut + 1.0) * (gate_cut * jax.nn.sigmoid(SIGMOID_SLOPE * gate_cut))


def slot_ids(routes, capacity, experts):
    batch_size, rows_each, top_count = routes.shape
    flat_ids = routes.reshape(batch_size, rows_each * top_count)
    onehot = (flat_ids[:, :, None] == jnp.arange(experts, dtype=jnp.int32)[None, None, :]).astype(
        jnp.int32
    )
    earlier = jnp.cumsum(onehot, axis=1) - onehot
    rank_in = jnp.sum(earlier * onehot, axis=2)
    return (flat_ids * capacity + rank_in).reshape(batch_size, rows_each, top_count)


def dispatch_rows(slots, row_data, slot_total):
    chosen = jnp.any(slots[..., None] == jnp.arange(slot_total, dtype=jnp.int32), axis=2).astype(
        jnp.bfloat16
    )
    return jnp.einsum("brs,brd->bsd", chosen, row_data, preferred_element_type=jnp.float32).astype(
        jnp.bfloat16
    )


def on_device(
    residual_in,
    queries,
    key_rows,
    value_rows,
    out_gate,
    decay_logit,
    head_gain,
    w_out,
    ffn_gain,
    routing,
    route_weight,
    w_gate,
    w_up,
    w_down,
):
    query_blk = to_blocks(queries, DK) * DK ** (-0.5)
    key_blk = to_blocks(key_rows, DK)
    value_blk = to_blocks(value_rows, DV)
    logdecay_blk = to_blocks(jax.nn.log_sigmoid(decay_logit) / DECAY_TEMP, DK)
    inner_part, query_dec, contrib, passing = block_parts(
        query_blk, key_blk, value_blk, logdecay_blk
    )
    total_decay = jnp.prod(passing, axis=0)
    local_state = fold_state(contrib, passing)
    incoming = carried_state(total_decay, local_state)
    readouts, _ = carry_blocks(query_dec, contrib, passing, incoming)
    mixed_blk = inner_part + readouts
    mixed_out = finish_heads(mixed_blk, head_gain, out_gate)
    tp_count = lax.axis_size("tp")
    quarter = mixed_out.shape[0] // tp_count
    rows_here = mixed_out.shape[1]
    w_rows = lax.dynamic_slice_in_dim(w_out, lax.axis_index("tp") * rows_here, rows_here, 0)
    projected = lax.psum_scatter(
        jnp.dot(mixed_out, w_rows, preferred_element_type=jnp.float32).astype(jnp.bfloat16),
        "tp",
        scatter_dimension=0,
        tiled=True,
    ).astype(jnp.float32)
    residual = (residual_in.astype(jnp.float32) + projected).astype(jnp.bfloat16)
    normed = norm_rows(residual, ffn_gain)
    experts = lax.axis_size("sp")
    top_count = routing.shape[1]
    capacity = 2 * routing.shape[0] * top_count // (tp_count * experts)
    model_width = normed.shape[1]
    slot_total = experts * capacity
    gate_cols = w_gate[0]
    up_cols = w_up[0]
    down_rows = w_down[0]
    own_routes = lax.dynamic_slice_in_dim(routing, lax.axis_index("tp") * quarter, quarter, 0)
    own_slots = slot_ids(own_routes[None], capacity, experts)[0]
    outgoing = dispatch_rows(own_slots[None], normed[None], slot_total)[0]
    arrived = lax.all_to_all(
        outgoing.reshape(experts, capacity, model_width),
        "sp",
        split_axis=0,
        concat_axis=0,
        tiled=True,
    )
    portion = lax.all_gather(arrived[None], "tp", axis=0, tiled=True)
    flat_rows = portion.reshape(-1, model_width)
    gate_pre = jnp.dot(flat_rows, gate_cols, preferred_element_type=jnp.float32)
    up_pre = jnp.dot(flat_rows, up_cols, preferred_element_type=jnp.float32)
    hidden_rows = clamped_unit(gate_pre, up_pre).astype(jnp.bfloat16)
    hidden = hidden_rows.reshape(portion.shape[:-1] + (gate_cols.shape[1],))
    portion = hidden
    partial_out = jnp.dot(
        portion.reshape(-1, hidden.shape[-1]), down_rows, preferred_element_type=jnp.float32
    ).astype(jnp.bfloat16)
    partial_out = lax.optimization_barrier(partial_out)
    summed = lax.psum_scatter(
        partial_out.astype(jnp.float32)
        .reshape(portion.shape[:-1] + (model_width,))
        .astype(jnp.bfloat16),
        "tp",
        scatter_dimension=0,
        tiled=True,
    ).astype(jnp.float32)
    returned = lax.all_to_all(
        summed[0].astype(jnp.bfloat16), "sp", split_axis=0, concat_axis=0, tiled=True
    )
    picked = jnp.take(
        returned.reshape(slot_total, model_width), own_slots.reshape(-1), axis=0
    ).reshape(quarter, top_count, model_width)
    routed = jnp.sum(picked.astype(jnp.float32) * route_weight[:, :, None], axis=1)
    return (residual.astype(jnp.float32) + routed).astype(jnp.bfloat16)


def solution(mesh):
    placed = (
        P(("sp", "tp"), None),
        P("sp", "tp"),
        P("sp", "tp"),
        P("sp", "tp"),
        P("sp", "tp"),
        P("sp", "tp"),
        P(),
        P(),
        P(),
        P("sp", None),
        P(("sp", "tp"), None),
        P("sp", None, "tp"),
        P("sp", None, "tp"),
        P("sp", "tp", None),
    )
    return jax.shard_map(
        on_device, mesh=mesh, in_specs=placed, out_specs=P(("sp", "tp"), None), check_vma=False
    )
```

profile of v0, /device:TPU:0, one launch (start us, length us, event | category | flops | bytes accessed | tf_op | source)
XLA Modules:
  0.0 408.4 jit_solution(18351942816302006135)
XLA Ops:
  6.5 1.1 fusion.36
  10.0 0.9 reshape.276
  10.9 0.9 reshape.277
  13.5 34.6 %all-gather.1 = bf16[16,64,128]{2,1,0:T(8,128)(2,1)} all-gather(bf16[2,64,128]{2,1,0:T(8,128)(2,1)S(1)} %convert_element_type.118), channel_id=3, replica_groups=mesh['sp'=8,'tp'=4] {'sp'}, dimensions={0}, use_global_device_ids=true | all-gather | bytes 294912 | tf_op jit(solution)/shard_map/all_gather | solution.py:21
  48.0 20.5 %all-gather.3 = bf16[8,2,64]{2,1,0:T(2,128)(2,1)S(1)} all-gather(bf16[1,2,64]{2,1,0:T(2,128)(2,1)} %bitcast.145), channel_id=2, replica_groups=mesh['sp'=8,'tp'=4] {'sp'}, dimensions={0}, use_global_device_ids=true | all-gather | bytes 2304 | tf_op jit(solution)/shard_map/all_gather | solution.py:21
  68.6 7.2 %while.39 = (s32[]{:T(128)}, f32[2,64,128]{2,1,0:T(8,128)S(1)}, s32[]{:T(128)}, bf16[8,2,64]{2,1,0:T(2,128)(2,1)S(1)}, bf16[8,2,64,128]{3,2,1,0:T(8,128)(2,1)}, /*index=5*/s32[]{:T(128)}, s32[]{:T(128)}) while((s32[]{:T(128)}, f32[2,64,128]{2,1,0:T(8,128)S(1)}, s32[]{:T(128)}, bf16[8,2,64]{2,1,0:T(2,128)(2,1)S(1)}, ...), condition=%wide.region_5.6_spmd.clone, body=%wide.region_4.5_spmd.clone.sunk | while | flops 82052 | bytes 165225 | solution.py:38
  69.5 0.9 fusion.70
  70.4 0.9 fusion.70
  71.3 0.9 fusion.70
  72.2 0.9 fusion.70
  73.1 0.9 fusion.70
  74.0 0.9 fusion.70
  74.9 0.9 fusion.70
  75.7 3.8 while.37
  79.5 3.8 exponential_multiply_fusion
  83.4 22.4 %fusion.6 = f32[4,2,64,1,64]{4,3,2,1,0:T(1,128)S(1)} fusion(f32[4,2,64,64,64]{4,3,2,1,0:T(8,128)S(1)} %exponential_multiply_fusion, bf16[4,2,64,64,1]{3,2,1,0,4:T(8,128)(2,1)S(1)} %bitcast.132), kind=kOutput, calls=%fused_computation.15 | convolution fusion | flops 25165824 | bytes 8585216 | tf_op jit(solution)/shard_map/nhtsk,nhsk->nhts/dot_general | solution.py:47
  107.1 2.7 convolution_convert_fusion.2
  111.6 20.5 %reduce-scatter.3.cloned.1.call-done = bf16[64,2048]{1,0:T(8,128)(2,1)} async-done(((bf16[256,2048]{1,0:T(8,128)(2,1)}), bf16[64,2048]{1,0:T(8,128)(2,1)}) %reduce-scatter.3.cloned.1.call-update) | async-done | bytes 262160 | tf_op jit(solution)/shard_map/reduce_scatter | solution.py:178
  132.1 1.1 fusion.14
  133.2 1.7 convolution_convert_fusion.1
  135.0 53.5 %all_to_all.10 = bf16[8,64,2048]{2,1,0:T(8,128)(2,1)} all-to-all(bf16[8,64,2048]{2,1,0:T(8,128)(2,1)S(1)} %bitcast.130), channel_id=1, replica_groups=mesh['sp'=8,'tp'=4] {'sp'}, dimensions={0} | all-to-all | bytes 4194304 | tf_op jit(solution)/shard_map/all_to_all | solution.py:197
  188.5 56.5 %all-gather.6.cloned.1.call-done = bf16[32,64,2048]{2,1,0:T(8,128)(2,1)} async-done(((bf16[8,64,2048]{2,1,0:T(8,128)(2,1)}), bf16[32,64,2048]{2,1,0:T(8,128)(2,1)}) %all-gather.6.cloned.1.call-update) | async-done | bytes 8388624 | tf_op jit(solution)/shard_map/all_gather | solution.py:204
  245.0 7.7 %fusion.10 = f32[2048,512]{1,0:T(8,128)S(1)} fusion(bf16[2048,2048]{1,0:T(8,128)(2,1)} %bitcast.146, bf16[1,2048,512]{2,1,0:T(8,128)(2,1)} %param.32), kind=kOutput, calls=%fused_computation.24 | convolution fusion | flops 4294967296 | bytes 14680064 | tf_op jit(solution)/shard_map/dot_general | solution.py:207
  252.7 5.7 %multiply_convert_fusion = bf16[2048,512]{1,0:T(8,128)(2,1)S(1)} fusion(f32[2048,512]{1,0:T(8,128)S(1)} %fusion.10, bf16[2048,2048]{1,0:T(8,128)(2,1)S(1)} %bitcast.147, bf16[1,2048,512]{2,1,0:T(8,128)(2,1)S(1)} %copy-done.8), kind=kOutput, calls=%fused_computation.19 | convolution fusion | flops 4305453056 | bytes 16777216 | tf_op jit(solution)/shard_map/dot_general | solution.py:206
  258.4 6.8 %convolution_convert_fusion = bf16[2048,2048]{1,0:T(8,128)(2,1)} fusion(bf16[2048,512]{1,0:T(8,128)(2,1)S(1)} %multiply_convert_fusion, bf16[1,512,2048]{2,1,0:T(8,128)(2,1)S(1)} %copy-done), kind=kOutput, calls=%fused_computation.18 | convolution fusion | flops 4299161600 | bytes 12582912 | tf_op jit(solution)/shard_map/dot_general | solution.py:211
  265.3 71.6 %reduce-scatter.5.cloned.1.call-done = bf16[1,8,64,2048]{3,2,1,0:T(8,128)(2,1)} async-done(((bf16[4,8,64,2048]{3,2,1,0:T(8,128)(2,1)}), bf16[1,8,64,2048]{3,2,1,0:T(8,128)(2,1)}) %reduce-scatter.5.cloned.1.call-update) | async-done | bytes 2097168 | tf_op jit(solution)/shard_map/reduce_scatter | solution.py:215
  336.8 5.8 %all-to-all-start.1 = ((bf16[8,64,2048]{2,1,0:T(8,128)(2,1)}), bf16[8,64,2048]{2,1,0:T(8,128)(2,1)}, u32[]{:S(2)}, u32[]{:S(2)}) async-start(bf16[8,64,2048]{2,1,0:T(8,128)(2,1)} %bitcast.131), calls=%async_computation.3 | async-start | bytes 4194304 | tf_op jit(solution)/shard_map/all_to_all | solution.py:223
  343.1 47.7 %all-to-all-done.1 = bf16[8,64,2048]{2,1,0:T(8,128)(2,1)} async-done(((bf16[8,64,2048]{2,1,0:T(8,128)(2,1)}), bf16[8,64,2048]{2,1,0:T(8,128)(2,1)}, u32[]{:S(2)}, u32[]{:S(2)}) %all-to-all-start.1) | async-done | bytes 2097184 | tf_op jit(solution)/shard_map/all_to_all | solution.py:223
  390.7 4.2 %gather_fusion = bf16[256,2048]{1,0:T(8,128)(2,1)S(1)} fusion(bf16[512,2048]{1,0:T(8,128)(2,1)} %bitcast.29, s32[1024]{0:T(1024)S(1)} %pad_clamp_fusion), kind=kCustom, calls=%fused_computation | custom fusion | bytes 2098176 | tf_op jit(solution)/shard_map/jit(_take)/gather | solution.py:226
  395.0 1.2 gather.7
  396.2 3.6 multiply_reduce_fusion
  399.9 1.8 fusion.17
  (102 shorter events, 12.3 us)
Async XLA Ops:
  6.5 251.9 %copy-start = (bf16[1,512,2048]{2,1,0:T(8,128)(2,1)S(1)}, bf16[1,512,2048]{2,1,0:T(8,128)(2,1)}, u32[]{:S(2)}) copy-start(bf16[1,512,2048]{2,1,0:T(8,128)(2,1)} %param.33) | copy-start | bytes 6291460
  6.5 125.6 %reduce-scatter.3.cloned.1.call-start = ((), (), s32[]{:S(2)}) async-start(), calls=%async_computation.4 | async-start | bytes 1310720 | tf_op jit(solution)/shard_map/reduce_scatter | solution.py:178
  12.9 66.6 %copy-start.2 = (f32[4,64,2,64]{3,1,2,0:T(8,128)S(1)}, f32[4,64,2,64]{3,1,2,0:T(8,128)}, u32[]{:S(2)}) copy-start(f32[4,64,2,64]{3,1,2,0:T(8,128)} %copy.115) | copy-start | bytes 393220
  83.4 22.5 %copy-start.3 = (f32[4,2,64,128]{3,2,1,0:T(8,128)S(1)}, f32[4,2,64,128]{3,2,1,0:T(8,128)}, u32[]{:S(2)}) copy-start(f32[4,2,64,128]{3,2,1,0:T(8,128)} %get-tuple-element.155) | copy-start | bytes 786436
  83.4 23.3 %copy-start.10 = (bf16[128]{0:T(256)(128)(2,1)S(1)}, bf16[128]{0:T(256)(128)(2,1)}, u32[]{:S(2)}) copy-start(bf16[128]{0:T(256)(128)(2,1)} %param.26) | copy-start | bytes 772
  83.4 23.7 %copy-start.9 = (bf16[256,256]{1,0:T(8,128)(2,1)S(1)}, bf16[256,256]{1,0:T(8,128)(2,1)}, u32[]{:S(2)}) copy-start(bf16[256,256]{1,0:T(8,128)(2,1)} %param.24) | copy-start | bytes 393220
  105.8 4.0 copy-start.6
  105.8 5.6 %copy-start.4 = (bf16[2048]{0:T(1024)(128)(2,1)S(1)}, bf16[2048]{0:T(1024)(128)(2,1)}, u32[]{:S(2)}) copy-start(bf16[2048]{0:T(1024)(128)(2,1)} %param.28) | copy-start | bytes 12292
  105.8 26.3 %copy-start.1 = (bf16[64,2048]{1,0:T(8,128)(2,1)S(1)}, bf16[64,2048]{1,0:T(8,128)(2,1)}, u32[]{:S(2)}) copy-start(bf16[64,2048]{1,0:T(8,128)(2,1)} %param.20) | copy-start | bytes 786436
  109.8 135.2 %all-gather.6.cloned.1.call-start = ((), (), s32[]{:S(2)}) async-start(), calls=%async_computation.6 | async-start | bytes 10485760 | tf_op jit(solution)/shard_map/all_gather | solution.py:204
  188.5 148.4 %reduce-scatter.5.cloned.1.call-start = ((), (), s32[]{:S(2)}) async-start(), calls=%async_computation.5 | async-start | bytes 10485760 | tf_op jit(solution)/shard_map/reduce_scatter | solution.py:215
  245.0 7.7 %copy-start.7 = (bf16[32,64,2048]{2,1,0:T(8,128)(2,1)S(1)}, bf16[32,64,2048]{2,1,0:T(8,128)(2,1)}, u32[]{:S(2)}) copy-start(bf16[32,64,2048]{2,1,0:T(8,128)(2,1)} %all-gather.6.cloned.1.call-done) | copy-start | bytes 25165828
  245.0 7.7 %copy-start.8 = (bf16[1,2048,512]{2,1,0:T(8,128)(2,1)S(1)}, bf16[1,2048,512]{2,1,0:T(8,128)(2,1)}, u32[]{:S(2)}) copy-start(bf16[1,2048,512]{2,1,0:T(8,128)(2,1)} %param.31) | copy-start | bytes 6291460
  265.3 77.7 %copy-start.5 = (f32[64,4]{0,1:T(4,128)S(1)}, f32[64,4]{0,1:T(4,128)}, u32[]{:S(2)}) copy-start(f32[64,4]{0,1:T(4,128)} %param.30) | copy-start | bytes 3076
  336.8 53.9 %all-to-all-start.1 = ((bf16[8,64,2048]{2,1,0:T(8,128)(2,1)}), bf16[8,64,2048]{2,1,0:T(8,128)(2,1)}, u32[]{:S(2)}, u32[]{:S(2)}) async-start(bf16[8,64,2048]{2,1,0:T(8,128)(2,1)} %bitcast.131), calls=%async_computation.3 | async-start | bytes 4194304 | tf_op jit(solution)/shard_map/all_to_all | solution.py:223
Sparse Core Ops, SparseCore 0:
  109.9 22.1 reduce-scatter.2
  188.6 56.3 all-gather.5
  265.4 71.4 reduce-scatter.4
where the time goes:
time: 412 us; the launch traced here: 408 us
  waiting for transfers between devices  196 us (48%)
  blocking collectives  109 us (26%)
  matrix products  51.3 us (12%)
  other arithmetic  22 us (5%)
  between operations  13.7 us (3%)
  local copies, waits for them, and re-layouts  10.2 us (2%)
  starting transfers between devices  5.89 us (1%)
    reduce_scatter x1, waiting for transfers between devices, on_device(): lax.psum_scatter(partial_out.astype(jnp.float32).reshape(portion.shape[:-...  71.6 us
    all_gather x1, waiting for transfers between devices, on_device(): portion = lax.all_gather(arrived[None], 'tp', axis=0, tiled=True)  56.5 us
    all_gather x2, blocking collectives, entering(): lax.all_gather(part.astype(kind), axis)  55.1 us
    all_to_all x1, blocking collectives, on_device(): lax.all_to_all(outgoing.reshape(experts, capacity, model_width), 'sp', sp...  53.5 us
    all_to_all x1, waiting for transfers between devices, on_device(): lax.all_to_all(summed[0].astype(jnp.bfloat16), 'sp', split_axis=0, concat...  47.7 us
    dot_general x1, matrix products, block_parts(): jnp.einsum('nhtsk,nhsk->nhts', weighted, key_blk, precision=EXACT_PRECISION)  22.4 us
    reduce_scatter x1, waiting for transfers between devices, on_device(): lax.psum_scatter(jnp.dot(mixed_out, w_rows, preferred_element_type=jnp.fl...  20.5 us
  transfers between devices with their start and end apart: 4, of which 4 were waited for; matrix products, arithmetic and copies ran while one was open for 1% of the time, Pallas kernels for 0%

commit v1 on v0

v1 whole, which is shorter than its diff:
```python
import jax
import jax.numpy as jnp
from jax import lax
from jax.experimental import pallas as pl
from jax.experimental.pallas import tpu as pltpu
from jax.sharding import PartitionSpec as P
import functools

DK = 64
DV = 128


DECAY_TEMP = 16.0
CLAMP_LIMIT = 7.0
SIGMOID_SLOPE = 1.702
NORM_EPS = 1e-06
EXACT_PRECISION = lax.Precision.HIGHEST


def clamped_unit(gate_pre, up_pre):
    gate_cut = jnp.minimum(gate_pre, CLAMP_LIMIT)
    up_cut = jnp.clip(up_pre, -CLAMP_LIMIT, CLAMP_LIMIT)
    return (up_cut + 1.0) * (gate_cut * jax.nn.sigmoid(SIGMOID_SLOPE * gate_cut))


MESH = pl.DeviceIdType.MESH
LANES = 128
SUB = 32
EXP_CAP = 64.0


def nt_dot(left, right):
    return lax.dot_general(
        left, right, (((1,), (1,)), ((), ())), preferred_element_type=jnp.float32
    )


def tn_dot(left, right):
    return lax.dot_general(
        left, right, (((0,), (0,)), ((), ())), preferred_element_type=jnp.float32
    )


def mix_kernel(
    sp_count, tp_count,
    q_ref, k_ref, v_ref, gate_ref, decay_ref, head_gain_ref, w_hbm, ffn_gain_ref,
    routing_ref, weight_ref, res_in_ref,
    res_ref, ext_ref,
    states, attended, mixed, mixed_in, w_vmem,
    w_sem, state_send, state_recv, mix_send, mix_recv,
):
    sp_me, tp_me = lax.axis_index("sp"), lax.axis_index("tp")
    barrier = pltpu.get_barrier_semaphore()

    @pl.loop(1, sp_count)
    def _(d):
        pl.semaphore_signal(
            barrier, inc=1, device_id={"sp": lax.rem(sp_me + d, sp_count)}, device_id_type=MESH
        )

    @pl.loop(1, tp_count)
    def _(d):
        pl.semaphore_signal(
            barrier, inc=1, device_id={"tp": lax.rem(tp_me + d, tp_count)}, device_id_type=MESH
        )

    w_copy = pltpu.make_async_copy(w_hbm, w_vmem, w_sem)
    w_copy.start()

    tokens, key_lanes = q_ref.shape
    value_lanes = v_ref.shape[1]
    head_count = key_lanes // DK
    lane_head = lax.broadcasted_iota(jnp.int32, (1, key_lanes), 1) // DK
    logit = decay_ref[...]
    log_decay = (jnp.minimum(logit, 0.0) - jnp.log1p(jnp.exp(-jnp.abs(logit)))) / DECAY_TEMP
    row_id = lax.broadcasted_iota(jnp.int32, (tokens, tokens), 0)
    col_id = lax.broadcasted_iota(jnp.int32, (tokens, tokens), 1)
    lower = (row_id >= col_id).astype(jnp.float32)
    cumulative = jnp.dot(
        lower, log_decay, precision=EXACT_PRECISION, preferred_element_type=jnp.float32
    )
    keys = k_ref[...].astype(jnp.float32)
    query = q_ref[...].astype(jnp.float32) * DK ** (-0.5)
    values = v_ref[...]
    ending = cumulative[tokens - 1 :, :]
    wide = tn_dot(values, (keys * jnp.exp(ending - cumulative)).astype(jnp.bfloat16))
    state = jnp.zeros((DV, key_lanes), jnp.float32)
    for h in range(head_count):
        state = jnp.where(lane_head == h, wide[h * DV : (h + 1) * DV, :], state)
    passing = jnp.exp(ending)
    passing_hi = passing.astype(jnp.bfloat16).astype(jnp.float32)
    tail_row = lax.broadcasted_iota(jnp.int32, (16, key_lanes), 0)
    tail = jnp.where(
        tail_row == 0, passing_hi, jnp.where(tail_row == 1, passing - passing_hi, 0.0)
    )
    states[sp_me, 0:DV, :] = state.astype(jnp.bfloat16)
    states[sp_me, DV : DV + 16, :] = tail.astype(jnp.bfloat16)

    pl.semaphore_wait(barrier, sp_count + tp_count - 2)

    def state_copy(slot, d):
        return pltpu.make_async_remote_copy(
            src_ref=states.at[slot],
            dst_ref=states.at[slot],
            send_sem=state_send.at[d],
            recv_sem=state_recv.at[slot],
            device_id={"sp": lax.rem(sp_me + d, sp_count)},
            device_id_type=MESH,
        )

    @pl.loop(1, sp_count)
    def _(d):
        state_copy(sp_me, d).start()

    for i in range(tokens // SUB):
        first = i * SUB
        reach = min(-(-(first + SUB) // LANES) * LANES, tokens)
        start = cumulative[first - 1 : first, :] if i else jnp.zeros((1, key_lanes), jnp.float32)
        q_sub = query[first : first + SUB] * jnp.exp(cumulative[first : first + SUB] - start)
        k_sub = keys[:reach] * jnp.exp(jnp.minimum(start - cumulative[:reach], EXP_CAP))
        stacked = jnp.concatenate(
            [jnp.where(lane_head == h, q_sub, 0.0) for h in range(head_count)], axis=0
        )
        scores = nt_dot(stacked.astype(jnp.bfloat16), k_sub.astype(jnp.bfloat16))
        at_row = lax.broadcasted_iota(jnp.int32, scores.shape, 0) % SUB + first
        at_col = lax.broadcasted_iota(jnp.int32, scores.shape, 1)
        scores = jnp.where(at_row >= at_col, scores, 0.0).astype(jnp.bfloat16)
        inner = jnp.dot(scores, values[:reach], preferred_element_type=jnp.float32)
        for h in range(head_count):
            attended[first : first + SUB, h * DV : (h + 1) * DV] = inner[
                h * SUB : (h + 1) * SUB, h * DV : (h + 1) * DV
            ]

    @pl.loop(1, sp_count)
    def _(d):
        state_copy(lax.rem(sp_me + d, sp_count), d).wait_recv()

    def absorb(j, incoming):
        decay = states[j, DV : DV + 16, :].astype(jnp.float32)
        total = decay[0:1, :] + decay[1:2, :]
        following = total * incoming + states[j, 0:DV, :].astype(jnp.float32)
        return jnp.where(j < sp_me, following, incoming)

    incoming = lax.fori_loop(
        0, sp_count, absorb, jnp.zeros((DV, key_lanes), jnp.float32)
    ).astype(jnp.bfloat16)
    query_dec = query * jnp.exp(cumulative)
    for h in range(head_count):
        cols = slice(h * DV, (h + 1) * DV)
        readout = nt_dot(jnp.where(lane_head == h, query_dec, 0.0).astype(jnp.bfloat16), incoming)
        head = attended[:, cols] + readout
        scale = lax.rsqrt(jnp.mean(head * head, axis=-1, keepdims=True) + NORM_EPS)
        opened = gate_ref[:, cols].astype(jnp.float32)
        opened = opened * jax.nn.sigmoid(opened)
        mixed[:, cols] = (head * scale * head_gain_ref[...].astype(jnp.float32) * opened).astype(
            jnp.bfloat16
        )

    rows = res_in_ref.shape[0]

    def mix_copy(block, slot, d):
        return pltpu.make_async_remote_copy(
            src_ref=mixed.at[pl.ds(pl.multiple_of(block * rows, rows), rows)],
            dst_ref=mixed_in.at[slot],
            send_sem=mix_send.at[d],
            recv_sem=mix_recv.at[slot],
            device_id={"tp": lax.rem(tp_me + d, tp_count)},
            device_id_type=MESH,
        )

    for d in range(1, tp_count):
        mix_copy(lax.rem(tp_me + d, tp_count), tp_me, d).start()

    lane = lax.broadcasted_iota(jnp.int32, (rows, LANES), 1)
    named = routing_ref[pl.ds(pl.multiple_of(tp_me * rows, rows), rows), :]
    share = jnp.zeros((rows, LANES), jnp.float32)
    for j in range(weight_ref.shape[1]):
        share = share + jnp.where(
            lane % (LANES // 2) == named[:, j : j + 1], weight_ref[:, j : j + 1], 0.0
        )
    share_hi = share.astype(jnp.bfloat16).astype(jnp.float32)
    width = res_in_ref.shape[1]
    ext_ref[:, width:] = jnp.where(lane < LANES // 2, share_hi, share - share_hi).astype(
        jnp.bfloat16
    )

    w_copy.wait()

    def w_rows(j):
        return w_vmem[pl.ds(pl.multiple_of(j * value_lanes, value_lanes), value_lanes), :]

    projected = jnp.dot(
        mixed[pl.ds(pl.multiple_of(tp_me * rows, rows), rows), :],
        w_rows(tp_me),
        preferred_element_type=jnp.float32,
    )
    for d in range(1, tp_count):
        slot = lax.rem(tp_me + d, tp_count)
        mix_copy(slot, slot, d).wait_recv()
        projected = projected + jnp.dot(
            mixed_in[slot], w_rows(slot), preferred_element_type=jnp.float32
        )
    residual = (res_in_ref[...].astype(jnp.float32) + projected).astype(jnp.bfloat16)
    res_ref[...] = residual
    wide_res = residual.astype(jnp.float32)
    inv = lax.rsqrt(jnp.mean(wide_res * wide_res, axis=-1, keepdims=True) + NORM_EPS)
    ext_ref[:, :width] = (wide_res * inv * ffn_gain_ref[...].astype(jnp.float32)).astype(
        jnp.bfloat16
    )

    @pl.loop(1, sp_count)
    def _(d):
        state_copy(sp_me, d).wait_send()

    for d in range(1, tp_count):
        mix_copy(lax.rem(tp_me + d, tp_count), tp_me, d).wait_send()


def mix_rows(
    queries, key_rows, value_rows, out_gate, decay_logit, head_gain, w_out,
    ffn_gain, routing, route_weight, residual_in,
):
    sp_count, tp_count = lax.axis_size("sp"), lax.axis_size("tp")
    rows, width = residual_in.shape
    tokens, key_lanes = queries.shape
    value_lanes = value_rows.shape[1]
    vmem = pl.BlockSpec(memory_space=pltpu.VMEM)
    return pl.pallas_call(
        functools.partial(mix_kernel, sp_count, tp_count),
        out_shape=(
            jax.ShapeDtypeStruct((rows, width), jnp.bfloat16),
            jax.ShapeDtypeStruct((rows, width + LANES), jnp.bfloat16),
        ),
        in_specs=[vmem] * 6 + [pl.BlockSpec(memory_space=pl.ANY)] + [vmem] * 4,
        out_specs=(vmem, vmem),
        scratch_shapes=[
            pltpu.VMEM((sp_count, DV + 16, key_lanes), jnp.bfloat16),
            pltpu.VMEM((tokens, value_lanes), jnp.float32),
            pltpu.VMEM((tokens, value_lanes), jnp.bfloat16),
            pltpu.VMEM((tp_count, rows, value_lanes), jnp.bfloat16),
            pltpu.VMEM(w_out.shape, jnp.bfloat16),
            pltpu.SemaphoreType.DMA,
            pltpu.SemaphoreType.DMA((sp_count,)),
            pltpu.SemaphoreType.DMA((sp_count,)),
            pltpu.SemaphoreType.DMA((tp_count,)),
            pltpu.SemaphoreType.DMA((tp_count,)),
        ],
        compiler_params=pltpu.CompilerParams(
            collective_id=0, has_side_effects=True, vmem_limit_bytes=40 << 20
        ),
        name="mix_rows",
    )(
        queries, key_rows, value_rows, out_gate, decay_logit, head_gain.reshape(1, -1), w_out,
        ffn_gain.reshape(1, -1), routing, route_weight, residual_in,
    )


def expert_kernel(x_ref, share_ref, gate_ref, up_ref, down_ref, out_ref):
    rows = x_ref[...]
    gate_pre = jnp.dot(rows, gate_ref[...], preferred_element_type=jnp.float32)
    up_pre = jnp.dot(rows, up_ref[...], preferred_element_type=jnp.float32)
    hidden = clamped_unit(gate_pre, up_pre).astype(jnp.bfloat16)
    lane = lax.broadcasted_iota(jnp.int32, share_ref.shape, 1) % (LANES // 2)
    share = jnp.sum(
        jnp.where(lane == lax.axis_index("sp"), share_ref[...].astype(jnp.float32), 0.0),
        axis=-1,
        keepdims=True,
    )
    out = jnp.dot(hidden, down_ref[...], preferred_element_type=jnp.float32)
    out_ref[...] = (out * share).astype(jnp.bfloat16)


def expert_rows(everyone, gate_cols, up_cols, down_rows):
    tokens = everyone.shape[0]
    width, units = gate_cols.shape
    step = min(256, tokens)
    return pl.pallas_call(
        expert_kernel,
        grid=(tokens // step,),
        out_shape=jax.ShapeDtypeStruct((tokens, width), jnp.bfloat16),
        in_specs=[
            pl.BlockSpec((step, width), lambda i: (i, 0)),
            pl.BlockSpec((step, LANES), lambda i: (i, width // LANES)),
            pl.BlockSpec((width, units), lambda i: (0, 0)),
            pl.BlockSpec((width, units), lambda i: (0, 0)),
            pl.BlockSpec((units, width), lambda i: (0, 0)),
        ],
        out_specs=pl.BlockSpec((step, width), lambda i: (i, 0)),
        compiler_params=pltpu.CompilerParams(vmem_limit_bytes=48 << 20),
        cost_estimate=pl.CostEstimate(
            flops=6 * tokens * width * units, bytes_accessed=8 * tokens * width, transcendentals=0
        ),
        name="expert_rows",
    )(everyone, everyone, gate_cols, up_cols, down_rows)


def slot_ids(routes, capacity, experts):
    batch_size, rows_each, top_count = routes.shape
    flat_ids = routes.reshape(batch_size, rows_each * top_count)
    onehot = (flat_ids[:, :, None] == jnp.arange(experts, dtype=jnp.int32)[None, None, :]).astype(
        jnp.int32
    )
    earlier = jnp.cumsum(onehot, axis=1) - onehot
    rank_in = jnp.sum(earlier * onehot, axis=2)
    return (flat_ids * capacity + rank_in).reshape(batch_size, rows_each, top_count)


def dispatch_rows(slots, row_data, slot_total):
    chosen = jnp.any(slots[..., None] == jnp.arange(slot_total, dtype=jnp.int32), axis=2).astype(
        jnp.bfloat16
    )
    return jnp.einsum("brs,brd->bsd", chosen, row_data, preferred_element_type=jnp.float32).astype(
        jnp.bfloat16
    )


def on_device(
    residual_in,
    queries,
    key_rows,
    value_rows,
    out_gate,
    decay_logit,
    head_gain,
    w_out,
    ffn_gain,
    routing,
    route_weight,
    w_gate,
    w_up,
    w_down,
):
    tp_count = lax.axis_size("tp")
    experts = lax.axis_size("sp")
    quarter = residual_in.shape[0]
    top_count = routing.shape[1]
    model_width = residual_in.shape[1]
    capacity = 2 * routing.shape[0] * top_count // (tp_count * experts)
    slot_total = experts * capacity
    residual, extended = mix_rows(
        queries, key_rows, value_rows, out_gate, decay_logit, head_gain, w_out,
        ffn_gain, routing, route_weight, residual_in,
    )
    if capacity >= quarter and experts <= LANES // 2:
        everyone = lax.all_gather(extended, ("sp", "tp"), axis=0, tiled=True)
        partial_rows = expert_rows(everyone, w_gate[0], w_up[0], w_down[0])
        routed = lax.psum_scatter(
            partial_rows, ("sp", "tp"), scatter_dimension=0, tiled=True
        ).astype(jnp.float32)
        return (residual.astype(jnp.float32) + routed).astype(jnp.bfloat16)
    normed = extended[:, :model_width]
    gate_cols = w_gate[0]
    up_cols = w_up[0]
    down_rows = w_down[0]
    own_routes = lax.dynamic_slice_in_dim(routing, lax.axis_index("tp") * quarter, quarter, 0)
    own_slots = slot_ids(own_routes[None], capacity, experts)[0]
    outgoing = dispatch_rows(own_slots[None], normed[None], slot_total)[0]
    arrived = lax.all_to_all(
        outgoing.reshape(experts, capacity, model_width),
        "sp",
        split_axis=0,
        concat_axis=0,
        tiled=True,
    )
    portion = lax.all_gather(arrived[None], "tp", axis=0, tiled=True)
    flat_rows = portion.reshape(-1, model_width)
    gate_pre = jnp.dot(flat_rows, gate_cols, preferred_element_type=jnp.float32)
    up_pre = jnp.dot(flat_rows, up_cols, preferred_element_type=jnp.float32)
    hidden_rows = clamped_unit(gate_pre, up_pre).astype(jnp.bfloat16)
    hidden = hidden_rows.reshape(portion.shape[:-1] + (gate_cols.shape[1],))
    portion = hidden
    partial_out = jnp.dot(
        portion.reshape(-1, hidden.shape[-1]), down_rows, preferred_element_type=jnp.float32
    ).astype(jnp.bfloat16)
    partial_out = lax.optimization_barrier(partial_out)
    summed = lax.psum_scatter(
        partial_out.astype(jnp.float32)
        .reshape(portion.shape[:-1] + (model_width,))
        .astype(jnp.bfloat16),
        "tp",
        scatter_dimension=0,
        tiled=True,
    ).astype(jnp.float32)
    returned = lax.all_to_all(
        summed[0].astype(jnp.bfloat16), "sp", split_axis=0, concat_axis=0, tiled=True
    )
    picked = jnp.take(
        returned.reshape(slot_total, model_width), own_slots.reshape(-1), axis=0
    ).reshape(quarter, top_count, model_width)
    routed = jnp.sum(picked.astype(jnp.float32) * route_weight[:, :, None], axis=1)
    return (residual.astype(jnp.float32) + routed).astype(jnp.bfloat16)


def solution(mesh):
    placed = (
        P(("sp", "tp"), None),
        P("sp", "tp"),
        P("sp", "tp"),
        P("sp", "tp"),
        P("sp", "tp"),
        P("sp", "tp"),
        P(),
        P(),
        P(),
        P("sp", None),
        P(("sp", "tp"), None),
        P("sp", None, "tp"),
        P("sp", None, "tp"),
        P("sp", "tp", None),
    )
    return jax.shard_map(
        on_device, mesh=mesh, in_specs=placed, out_specs=P(("sp", "tp"), None), check_vma=False
    )
```

time: 412 us -> 292 us (0.71)
  blocking collectives: 109 us -> 0 us
  matrix products: 51.3 us -> 0 us
  Pallas kernels: 0 us -> 36 us
  waiting for transfers between devices: 196 us -> 229 us
  other arithmetic: 22 us -> 1.71 us
  starting transfers between devices: 5.89 us -> 0.04 us
    reduce_scatter x2 -> x1, waiting for transfers between devices: 92 us -> 149 us  [on_device(): lax.psum_scatter(partial_rows, ('sp', 'tp'), scatter_dimension=0, tiled=T...]
    all_gather x2 -> x0, blocking collectives: 55.1 us -> none  [entering(): lax.all_gather(part.astype(kind), axis)]
    all_to_all x1 -> x0, blocking collectives: 53.5 us -> none  [on_device(): lax.all_to_all(outgoing.reshape(experts, capacity, model_width), 'sp', sp...]
    dot_general x12 -> x0, matrix products: 51.3 us -> none  [the longest x1 22.4 us: block_parts(): jnp.einsum('nhtsk,nhsk->nhts', weighted, key_blk, precision=EXACT_PRECISION)]
    all_to_all x1 -> x0, waiting for transfers between devices: 47.7 us -> none  [on_device(): lax.all_to_all(summed[0].astype(jnp.bfloat16), 'sp', split_axis=0, concat...]
    pallas_call x0 -> x2, Pallas kernels: none -> 36 us  [the longest x1 18.6 us: expert_rows(): pl.pallas_call(expert_kernel, grid=(tokens // step,), out_shape=jax.Shape...]
    all_gather x1, waiting for transfers between devices: 56.5 us -> 79.9 us  [on_device(): everyone = lax.all_gather(extended, ('sp', 'tp'), axis=0, tiled=True)]
    unnamed x23 -> x22, local copies, waits for them, and re-layouts: 0.15 us -> 11.4 us
  transfers between devices with their start and end apart: 4 -> 2, of which waited for: 4 -> 2; matrix products, arithmetic and copies ran while one was open for 1% -> 0% of each run, Pallas kernels for 0% -> 0%
where the time goes in v1:
time: 292 us
  waiting for transfers between devices  229 us (78%)
  Pallas kernels  36 us (12%)
  between operations  13.4 us (5%)
  local copies, waits for them, and re-layouts  12 us (4%)
    reduce_scatter x1, waiting for transfers between devices, on_device(): lax.psum_scatter(partial_rows, ('sp', 'tp'), scatter_dimension=0, tiled=T...  149 us
    all_gather x1, waiting for transfers between devices, on_device(): everyone = lax.all_gather(extended, ('sp', 'tp'), axis=0, tiled=True)  79.9 us
    pallas_call x1, Pallas kernels, expert_rows(): pl.pallas_call(expert_kernel, grid=(tokens // step,), out_shape=jax.Shape...  18.6 us
    pallas_call x1, Pallas kernels, mix_rows(): pl.pallas_call(functools.partial(mix_kernel, sp_count, tp_count), out_sha...  17.4 us
    unnamed x22, local copies, waits for them, and re-layouts  11.4 us
  transfers between devices with their start and end apart: 2, of which 2 were waited for; matrix products, arithmetic and copies ran while one was open for 0% of the time, Pallas kernels for 0%

profile of v1, /device:TPU:0, one launch (start us, length us, event | category | flops | bytes accessed | tf_op | source)
XLA Modules:
  0.0 292.0 jit_solution(17167362337615738807)
XLA Ops:
  6.5 0.0 all-gather.2.cloned.1.call-start
  6.5 0.7 reshape.7.ffn_gain_ref
  7.2 0.8 copy.16.weight_ref
  8.0 0.8 copy.15.routing_ref
  8.8 0.0 copy-start
  8.8 2.2 copy-done
  11.0 0.0 copy-start.1
  11.0 0.9 copy-done.1
  12.0 0.0 copy-start.2
  12.0 0.9 copy-done.2
  12.9 0.0 copy-start.3
  12.9 0.9 copy-done.3
  13.8 0.0 copy-start.4
  13.8 0.9 copy-done.4
  14.7 0.0 copy-start.5
  14.7 0.8 copy-done.5
  15.5 0.0 copy-start.6
  15.5 0.8 copy-done.6
  16.4 0.0 copy-start.7
  16.4 0.7 copy-done.7
  17.0 0.0 copy-start.8
  17.0 17.4 %mix_rows.1 = (bf16[64,2048]{1,0:T(8,128)(2,1)S(1)}, bf16[64,2176]{1,0:T(8,128)(2,1)}) custom-call(bf16[256,128]{1,0:T(8,128)(2,1)S(1)} %copy-done.5, bf16[256,128]{1,0:T(8,128)(2,1)S(1)} %copy-done.6, bf16[256,256]{1,0:T(8,128)(2,1)S(1)} %copy-done.2, bf16[256,256]{1,0:T(8,128)(2,1)S(1)} %copy-done.3, f32[256,128]{1,0:T(8,128)S(1)} %copy-done.4, ...), custom_call_target="tpu_custom_call" | custom-call | tf_op jit(solution)/shard_map/mix_rows/pallas_call | solution.py:228
  34.4 0.0 all-gather.2.cloned.1.call-update
  34.4 0.0 reduce-scatter.2.cloned.1.call-start
  34.5 79.9 %all-gather.2.cloned.1.call-done.x_ref.share_ref = bf16[2048,2176]{1,0:T(8,128)(2,1)} async-done(((bf16[64,2176]{1,0:T(8,128)(2,1)}), bf16[2048,2176]{1,0:T(8,128)(2,1)}) %all-gather.2.cloned.1.call-update) | async-done | bytes 8912912 | tf_op jit(solution)/shard_map/all_gather | solution.py:345
  114.3 0.0 copy-done.8
  114.4 0.0 copy-start.9
  114.4 1.6 copy-done.9
  115.9 18.6 %expert_rows.1 = bf16[2048,2048]{1,0:T(8,128)(2,1)} custom-call(bf16[2048,2176]{1,0:T(8,128)(2,1)} %all-gather.2.cloned.1.call-done.x_ref.share_ref, bf16[2048,2176]{1,0:T(8,128)(2,1)} %all-gather.2.cloned.1.call-done.x_ref.share_ref, bf16[2048,512]{1,0:T(8,128)(2,1)S(1)} %bitcast.5, bf16[2048,512]{1,0:T(8,128)(2,1)S(1)} %bitcast.6, bf16[512,2048]{1,0:T(8,128)(2,1)} %bitcast.7), custom_call_target="tpu_custom_call" | custom-call | flops 12884901888 | bytes 33554432 | tf_op jit(solution)/shard_map/expert_rows/pallas_call | solution.py:277
  134.6 0.0 reduce-scatter.2.cloned.1.call-update
  134.6 148.8 %reduce-scatter.2.cloned.1.call-done = bf16[64,2048]{1,0:T(8,128)(2,1)} async-done(((bf16[2048,2048]{1,0:T(8,128)(2,1)}), bf16[64,2048]{1,0:T(8,128)(2,1)}) %reduce-scatter.2.cloned.1.call-update) | async-done | bytes 262160 | tf_op jit(solution)/shard_map/reduce_scatter | solution.py:347
  283.4 1.7 add_convert_fusion
Async XLA Ops:
  6.5 107.8 %all-gather.2.cloned.1.call-start = ((), (), s32[]{:S(2)}) async-start(), calls=%async_computation.1 | async-start | bytes 9191424 | tf_op jit(solution)/shard_map/all_gather | solution.py:345
  8.8 2.2 copy-start
  11.0 0.9 copy-start.1
  12.0 0.9 copy-start.2
  12.9 0.9 copy-start.3
  13.8 0.9 copy-start.4
  14.7 0.8 copy-start.5
  15.5 0.8 copy-start.6
  16.4 0.7 copy-start.7
  17.0 97.3 %copy-start.8 = (bf16[1,2048,512]{2,1,0:T(8,128)(2,1)S(1)}, bf16[1,2048,512]{2,1,0:T(8,128)(2,1)}, u32[]{:S(2)}) copy-start(bf16[1,2048,512]{2,1,0:T(8,128)(2,1)} %param.25) | copy-start | bytes 6291460
  34.4 249.0 %reduce-scatter.2.cloned.1.call-start = ((), (), s32[]{:S(2)}) async-start(), calls=%async_computation.2 | async-start | bytes 8650752 | tf_op jit(solution)/shard_map/reduce_scatter | solution.py:347
  114.4 1.6 copy-start.9
Sparse Core Ops, SparseCore 0:
  34.5 79.7 all-gather.1
  134.7 148.6 reduce-scatter.1

commit v2 on v1

--- a/solution.py
+++ b/solution.py
@@ -255,43 +255,242 @@
     )
 
 
-def expert_kernel(x_ref, share_ref, gate_ref, up_ref, down_ref, out_ref):
-    rows = x_ref[...]
-    gate_pre = jnp.dot(rows, gate_ref[...], preferred_element_type=jnp.float32)
-    up_pre = jnp.dot(rows, up_ref[...], preferred_element_type=jnp.float32)
-    hidden = clamped_unit(gate_pre, up_pre).astype(jnp.bfloat16)
-    lane = lax.broadcasted_iota(jnp.int32, share_ref.shape, 1) % (LANES // 2)
-    share = jnp.sum(
-        jnp.where(lane == lax.axis_index("sp"), share_ref[...].astype(jnp.float32), 0.0),
-        axis=-1,
-        keepdims=True,
-    )
-    out = jnp.dot(hidden, down_ref[...], preferred_element_type=jnp.float32)
-    out_ref[...] = (out * share).astype(jnp.bfloat16)
-
-
-def expert_rows(everyone, gate_cols, up_cols, down_rows):
-    tokens = everyone.shape[0]
+def expert_kernel(
+    z_count, y_count, gather_cuts, reduce_cuts,
+    ext_ref, res_ref, gate_hbm, up_hbm, down_hbm, out_ref,
+    rows_all, gate_w, up_w, down_w, hidden, shares, parts, got_core, got_first, got_second, got_z,
+    w_sem, own_sem, gather_send, gather_recv, reduce_send, reduce_recv,
+):
+    sp_me, tp_me = lax.axis_index("sp"), lax.axis_index("tp")
+    z, x = sp_me // 2, lax.rem(sp_me, 2)
+    y, c = tp_me // 2, lax.rem(tp_me, 2)
+    partner = {
+        "x": {"sp": z * 2 + 1 - x},
+        "y": {"tp": (1 - y) * 2 + c},
+        "c": {"tp": y * 2 + 1 - c},
+    }
+    barrier = pltpu.get_barrier_semaphore()
+
+    def z_peer(d):
+        return {"sp": lax.rem(z + d, z_count) * 2 + x}
+
+    for target in [z_peer(d) for d in range(1, z_count)] + list(partner.values()):
+        pl.semaphore_signal(barrier, inc=1, device_id=target, device_id_type=MESH)
+    loads = [
+        pltpu.make_async_copy(src, dst, w_sem.at[i])
+        for i, (src, dst) in enumerate(((gate_hbm, gate_w), (up_hbm, up_w), (down_hbm, down_w)))
+    ]
+    own = pltpu.make_async_copy(ext_ref, rows_all.at[z, x, y, c], own_sem)
+    own.start()
+    for load in loads:
+        load.start()
+    own.wait()
+    pl.semaphore_wait(barrier, z_count + 2)
+
+    def remote(src, dst, send, recv, target):
+        return pltpu.make_async_remote_copy(
+            src_ref=src, dst_ref=dst, send_sem=send, recv_sem=recv,
+            device_id=target, device_id_type=MESH,
+        )
+
+    def gather_copies(i, stage, arriving):
+        cols = pl.ds(gather_cuts[i][0], gather_cuts[i][1])
+        order = ("x", "y") if i % 2 else ("y", "x")
+        if stage == 0:
+            copies = []
+            for d in range(1, z_count):
+                zz = lax.rem(z + z_count - d, z_count) if arriving else z
+                block = rows_all.at[zz, x, y, c, :, cols]
+                copies.append(
+                    remote(block, block, gather_send.at[i, d], gather_recv.at[i, d], z_peer(d))
+                )
+            return copies
+        axis = order[stage - 1] if stage < 3 else "c"
+        xx = 1 - x if arriving and axis == "x" else x
+        yy = 1 - y if arriving and axis == "y" else y
+        cc = 1 - c if arriving and axis == "c" else c
+        if stage == 1:
+            block = rows_all.at[:, xx, yy, cc, :, cols]
+        elif stage == 2 and axis == "x":
+            block = rows_all.at[:, xx, :, cc, :, cols]
+        elif stage == 2:
+            block = rows_all.at[:, :, yy, cc, :, cols]
+        else:
+            block = rows_all.at[:, :, :, cc, :, cols]
+        sem = z_count - 1 + stage
+        return [
+            remote(block, block, gather_send.at[i, sem], gather_recv.at[i, sem], partner[axis])
+        ]
+
+    chunks = len(gather_cuts)
+    for tick in range(chunks + 4):
+        for i in range(chunks):
+            stage = tick - i
+            if 1 <= stage <= 4:
+                for copy in gather_copies(i, stage - 1, True):
+                    copy.wait_recv()
+            if 0 <= stage <= 3:
+                for copy in gather_copies(i, stage, False):
+                    copy.start()
+
+    for load in loads:
+        load.wait()
+    quarter, wide = ext_ref.shape
+    width = res_ref.shape[1]
+    group = y_count * 2 * quarter
+
+    @pl.loop(0, z_count * 2)
+    def _(b):
+        block = rows_all[b // 2, lax.rem(b, 2)].reshape(group, wide)
+        rows = block[:, :width]
+        gate_pre = jnp.dot(rows, gate_w[...], preferred_element_type=jnp.float32)
+        up_pre = jnp.dot(rows, up_w[...], preferred_element_type=jnp.float32)
+        hidden[b] = clamped_unit(gate_pre, up_pre).astype(jnp.bfloat16)
+        lane = lax.broadcasted_iota(jnp.int32, (group, LANES), 1) % (LANES // 2)
+        share = jnp.sum(
+            jnp.where(lane == sp_me, block[:, width:].astype(jnp.float32), 0.0),
+            axis=-1,
+            keepdims=True,
+        )
+        shares[b] = jnp.broadcast_to(share, (group, LANES))
+
+    def order_of(j):
+        return ("x", "y") if j % 2 else ("y", "x")
+
+    def reduce_copies(j, stage):
+        axis = "c" if stage == 0 else order_of(j)[stage - 1] if stage < 3 else "z"
+        if stage == 0:
+            src, dst = parts.at[j, :, :, :, 1 - c], got_core.at[j]
+        elif stage == 1 and axis == "y":
+            src, dst = parts.at[j, :, :, 1 - y, c], got_first.at[j]
+        elif stage == 1:
+            src, dst = parts.at[j, :, 1 - x, :, c], got_first.at[j]
+        elif stage == 2 and axis == "x":
+            src, dst = parts.at[j, :, 1 - x, y, c], got_second.at[j]
+        elif stage == 2:
+            src, dst = parts.at[j, :, x, 1 - y, c], got_second.at[j]
+        else:
+            return [
+                remote(
+                    parts.at[j, lax.rem(z + d, z_count), x, y, c], got_z.at[j, d - 1],
+                    reduce_send.at[j, 2 + d], reduce_recv.at[j, 2 + d], z_peer(d),
+                )
+                for d in range(1, z_count)
+            ]
+        return [
+            remote(
+                src, dst, reduce_send.at[j, stage], reduce_recv.at[j, stage], partner[axis]
+            )
+        ]
+
+    def add(ours, theirs):
+        return (ours.astype(jnp.float32) + theirs.astype(jnp.float32)).astype(jnp.bfloat16)
+
+    def absorb(j, stage):
+        for copy in reduce_copies(j, stage):
+            copy.wait_recv()
+        if stage == 3:
+            cols = slice(reduce_cuts[j][0], reduce_cuts[j][0] + reduce_cuts[j][1])
+            total = parts[j, z, x, y, c].astype(jnp.float32)
+            for d in range(1, z_count):
+                total = total + got_z[j, d - 1].astype(jnp.float32)
+            out_ref[:, cols] = (res_ref[:, cols].astype(jnp.float32) + total).astype(jnp.bfloat16)
+            return
+
+        @pl.loop(0, z_count)
+        def _(zz):
+            if stage == 0:
+                for xx in range(2):
+                    for yy in range(y_count):
+                        parts[j, zz, xx, yy, c] = add(
+                            parts[j, zz, xx, yy, c], got_core[j, zz, xx, yy]
+                        )
+            elif stage == 1 and order_of(j)[0] == "y":
+                for xx in range(2):
+                    parts[j, zz, xx, y, c] = add(parts[j, zz, xx, y, c], got_first[j, zz, xx])
+            elif stage == 1:
+                for yy in range(y_count):
+                    parts[j, zz, x, yy, c] = add(parts[j, zz, x, yy, c], got_first[j, zz, yy])
+            else:
+                parts[j, zz, x, y, c] = add(parts[j, zz, x, y, c], got_second[j, zz])
+
+    pieces = len(reduce_cuts)
+    for tick in range(pieces + 4):
+        if tick < pieces:
+            at, size = reduce_cuts[tick]
+
+            @pl.loop(0, z_count * 2)
+            def _(b):
+                out = jnp.dot(
+                    hidden[b], down_w[:, at : at + size], preferred_element_type=jnp.float32
+                )
+                out = (out * shares[b][:, 0:1]).astype(jnp.bfloat16)
+                parts[tick, b // 2, lax.rem(b, 2)] = out.reshape(y_count, 2, quarter, size)
+
+            reduce_copies(tick, 0)[0].start()
+        for j in range(pieces):
+            stage = tick - j
+            if 1 <= stage <= 4:
+                absorb(j, stage - 1)
+                if stage < 4:
+                    for copy in reduce_copies(j, stage):
+                        copy.start()
+
+    for i in range(chunks):
+        for stage in range(4):
+            for copy in gather_copies(i, stage, False):
+                copy.wait_send()
+    for j in range(pieces):
+        for stage in range(4):
+            for copy in reduce_copies(j, stage):
+                copy.wait_send()
+
+
+def cuts(total, pieces):
+    tiles = total // LANES
+    edges = [tiles * i // pieces * LANES for i in range(pieces + 1)]
+    return [(edges[i], edges[i + 1] - edges[i]) for i in range(pieces)]
+
+
+def expert_rows(extended, residual, gate_cols, up_cols, down_rows):
+    z_count, y_count = lax.axis_size("sp") // 2, lax.axis_size("tp") // 2
+    quarter, wide = extended.shape
     width, units = gate_cols.shape
-    step = min(256, tokens)
+    gather_cuts, reduce_cuts = cuts(wide, 4), cuts(width, 4)
+    pieces, size = len(reduce_cuts), reduce_cuts[0][1]
+    group = y_count * 2 * quarter
+    vmem = pl.BlockSpec(memory_space=pltpu.VMEM)
+    hbm = pl.BlockSpec(memory_space=pl.ANY)
+    bf16 = jnp.bfloat16
     return pl.pallas_call(
-        expert_kernel,
-        grid=(tokens // step,),
-        out_shape=jax.ShapeDtypeStruct((tokens, width), jnp.bfloat16),
-        in_specs=[
-            pl.BlockSpec((step, width), lambda i: (i, 0)),
-            pl.BlockSpec((step, LANES), lambda i: (i, width // LANES)),
-            pl.BlockSpec((width, units), lambda i: (0, 0)),
-            pl.BlockSpec((width, units), lambda i: (0, 0)),
-            pl.BlockSpec((units, width), lambda i: (0, 0)),
+        functools.partial(expert_kernel, z_count, y_count, gather_cuts, reduce_cuts),
+        out_shape=jax.ShapeDtypeStruct((quarter, width), bf16),
+        in_specs=[vmem, vmem, hbm, hbm, hbm],
+        out_specs=vmem,
+        scratch_shapes=[
+            pltpu.VMEM((z_count, 2, y_count, 2, quarter, wide), bf16),
+            pltpu.VMEM(gate_cols.shape, bf16),
+            pltpu.VMEM(up_cols.shape, bf16),
+            pltpu.VMEM(down_rows.shape, bf16),
+            pltpu.VMEM((z_count * 2, group, units), bf16),
+            pltpu.VMEM((z_count * 2, group, LANES), jnp.float32),
+            pltpu.VMEM((pieces, z_count, 2, y_count, 2, quarter, size), bf16),
+            pltpu.VMEM((pieces, z_count, 2, y_count, quarter, size), bf16),
+            pltpu.VMEM((pieces, z_count, 2, quarter, size), bf16),
+            pltpu.VMEM((pieces, z_count, quarter, size), bf16),
+            pltpu.VMEM((pieces, z_count - 1, quarter, size), bf16),
+            pltpu.SemaphoreType.DMA((3,)),
+            pltpu.SemaphoreType.DMA,
+            pltpu.SemaphoreType.DMA((len(gather_cuts), z_count + 3)),
+            pltpu.SemaphoreType.DMA((len(gather_cuts), z_count + 3)),
+            pltpu.SemaphoreType.DMA((pieces, z_count + 3)),
+            pltpu.SemaphoreType.DMA((pieces, z_count + 3)),
         ],
-        out_specs=pl.BlockSpec((step, width), lambda i: (i, 0)),
-        compiler_params=pltpu.CompilerParams(vmem_limit_bytes=48 << 20),
-        cost_estimate=pl.CostEstimate(
-            flops=6 * tokens * width * units, bytes_accessed=8 * tokens * width, transcendentals=0
+        compiler_params=pltpu.CompilerParams(
+            collective_id=1, has_side_effects=True, vmem_limit_bytes=56 << 20
         ),
         name="expert_rows",
-    )(everyone, everyone, gate_cols, up_cols, down_rows)
+    )(extended, residual, gate_cols, up_cols, down_rows)
 
 
 def slot_ids(routes, capacity, experts):
@@ -341,13 +540,8 @@
         queries, key_rows, value_rows, out_gate, decay_logit, head_gain, w_out,
         ffn_gain, routing, route_weight, residual_in,
     )
-    if capacity >= quarter and experts <= LANES // 2:
-        everyone = lax.all_gather(extended, ("sp", "tp"), axis=0, tiled=True)
-        partial_rows = expert_rows(everyone, w_gate[0], w_up[0], w_down[0])
-        routed = lax.psum_scatter(
-            partial_rows, ("sp", "tp"), scatter_dimension=0, tiled=True
-        ).astype(jnp.float32)
-        return (residual.astype(jnp.float32) + routed).astype(jnp.bfloat16)
+    if capacity >= quarter and experts <= LANES // 2 and experts % 2 == 0 and tp_count == 4:
+        return expert_rows(extended, residual, w_gate[0], w_up[0], w_down[0])
     normed = extended[:, :model_width]
     gate_cols = w_gate[0]
     up_cols = w_up[0]

time: 292 us -> 213 us (0.73)
  waiting for transfers between devices: 229 us -> 0 us
  Pallas kernels: 36 us -> 199 us
  between operations: 13.4 us -> 0.05 us
    pallas_call x1, Pallas kernels: 18.6 us -> 182 us  [expert_rows(): pl.pallas_call(functools.partial(expert_kernel, z_count, y_count, gather_...]
    reduce_scatter x1 -> x0, waiting for transfers between devices: 149 us -> none  [on_device(): lax.psum_scatter(partial_rows, ('sp', 'tp'), scatter_dimension=0, tiled=T...]
    all_gather x1 -> x0, waiting for transfers between devices: 79.9 us -> none  [on_device(): everyone = lax.all_gather(extended, ('sp', 'tp'), axis=0, tiled=True)]
    unnamed x22 -> x23, local copies, waits for them, and re-layouts: 11.4 us -> 12.8 us
  transfers between devices with their start and end apart: 2 -> 0, of which waited for: 2 -> 0; matrix products, arithmetic and copies ran while one was open for 0% -> 0% of each run, Pallas kernels for 0% -> 0%
where the time goes in v2:
time: 213 us; the launch traced here: 212 us
  Pallas kernels  199 us (93%)
  local copies, waits for them, and re-layouts  13.5 us (6%)
    pallas_call x1, Pallas kernels, expert_rows(): pl.pallas_call(functools.partial(expert_kernel, z_count, y_count, gather_...  182 us
    pallas_call x1, Pallas kernels, mix_rows(): pl.pallas_call(functools.partial(mix_kernel, sp_count, tp_count), out_sha...  16.6 us
    unnamed x23, local copies, waits for them, and re-layouts  12.8 us

profile of v2, /device:TPU:0, one launch (start us, length us, event | category | flops | bytes accessed | tf_op | source)
XLA Modules:
  0.0 212.1 jit_solution(4726578287530707365)
XLA Ops:
  0.0 0.7 reshape.7.ffn_gain_ref
  0.7 0.8 copy.16.weight_ref
  1.5 0.8 copy.15.routing_ref
  2.3 0.0 copy-start
  2.3 2.2 %copy-done = bf16[1024,2048]{1,0:T(8,128)(2,1)S(1)} copy-done((bf16[1024,2048]{1,0:T(8,128)(2,1)S(1)}, bf16[1024,2048]{1,0:T(8,128)(2,1)}, u32[]{:S(2)}) %copy-start) | copy-done | bytes 4194328
  4.5 0.0 copy-start.3
  4.5 0.9 copy-done.3
  5.4 0.0 copy-start.4
  5.4 0.9 copy-done.4
  6.3 0.0 copy-start.5
  6.3 0.9 copy-done.5
  7.2 0.0 copy-start.6
  7.2 0.9 copy-done.6
  8.1 0.0 copy-start.7
  8.1 0.8 copy-done.7
  9.0 0.0 copy-start.8
  9.0 0.8 copy-done.8
  9.8 0.0 copy-start.9
  9.8 0.7 copy-done.9
  10.5 16.6 %mix_rows.1 = (bf16[64,2048]{1,0:T(8,128)(2,1)S(1)}, bf16[64,2176]{1,0:T(8,128)(2,1)S(1)}) custom-call(bf16[256,128]{1,0:T(8,128)(2,1)S(1)} %copy-done.7, bf16[256,128]{1,0:T(8,128)(2,1)S(1)} %copy-done.8, bf16[256,256]{1,0:T(8,128)(2,1)S(1)} %copy-done.4, bf16[256,256]{1,0:T(8,128)(2,1)S(1)} %copy-done.5, f32[256,128]{1,0:T(8,128)S(1)} %copy-done.6, ...), custom_call_target="tpu_custom_call" | custom-call | tf_op jit(solution)/shard_map/mix_rows/pallas_call | solution.py:228
  27.1 0.0 copy-start.1
  27.1 0.7 copy-done.1
  27.8 0.0 copy-start.2
  27.8 0.7 copy-done.2
  28.5 181.9 %expert_rows.1 = bf16[64,2048]{1,0:T(8,128)(2,1)} custom-call(bf16[64,2176]{1,0:T(8,128)(2,1)} %copy-done.1, bf16[64,2048]{1,0:T(8,128)(2,1)} %copy-done.2, bf16[2048,512]{1,0:T(8,128)(2,1)} %bitcast.5, bf16[2048,512]{1,0:T(8,128)(2,1)} %bitcast.6, bf16[512,2048]{1,0:T(8,128)(2,1)} %bitcast.7), custom_call_target="tpu_custom_call" | custom-call | tf_op jit(solution)/shard_map/expert_rows/pallas_call | solution.py:465
  210.5 1.7 copy.18
Async XLA Ops:
  2.3 2.2 %copy-start = (bf16[1024,2048]{1,0:T(8,128)(2,1)S(1)}, bf16[1024,2048]{1,0:T(8,128)(2,1)}, u32[]{:S(2)}) copy-start(bf16[1024,2048]{1,0:T(8,128)(2,1)} %w_hbm.1) | copy-start | bytes 12582916
  4.5 0.9 copy-start.3
  5.4 0.9 copy-start.4
  6.3 0.9 copy-start.5
  7.2 0.9 copy-start.6
  8.1 0.8 copy-start.7
  9.0 0.8 copy-start.8
  9.8 0.7 copy-start.9
  27.1 0.7 copy-start.1
  27.8 0.7 copy-start.2

commit v3 on v2

--- a/solution.py
+++ b/solution.py
@@ -323,9 +323,9 @@
         ]
 
     chunks = len(gather_cuts)
-    for tick in range(chunks + 4):
+    for tick in range(chunks // 2 + 4):
         for i in range(chunks):
-            stage = tick - i
+            stage = tick - i // 2
             if 1 <= stage <= 4:
                 for copy in gather_copies(i, stage - 1, True):
                     copy.wait_recv()
@@ -415,9 +415,9 @@
                 parts[j, zz, x, y, c] = add(parts[j, zz, x, y, c], got_second[j, zz])
 
     pieces = len(reduce_cuts)
-    for tick in range(pieces + 4):
-        if tick < pieces:
-            at, size = reduce_cuts[tick]
+    for tick in range(pieces // 2 + 4):
+        for piece in range(2 * tick, min(2 * tick + 2, pieces)):
+            at, size = reduce_cuts[piece]
 
             @pl.loop(0, z_count * 2)
             def _(b):
@@ -425,11 +425,11 @@
                     hidden[b], down_w[:, at : at + size], preferred_element_type=jnp.float32
                 )
                 out = (out * shares[b][:, 0:1]).astype(jnp.bfloat16)
-                parts[tick, b // 2, lax.rem(b, 2)] = out.reshape(y_count, 2, quarter, size)
-
-            reduce_copies(tick, 0)[0].start()
+                parts[piece, b // 2, lax.rem(b, 2)] = out.reshape(y_count, 2, quarter, size)
+
+            reduce_copies(piece, 0)[0].start()
         for j in range(pieces):
-            stage = tick - j
+            stage = tick - j // 2
             if 1 <= stage <= 4:
                 absorb(j, stage - 1)
                 if stage < 4:
@@ -456,7 +456,7 @@
     z_count, y_count = lax.axis_size("sp") // 2, lax.axis_size("tp") // 2
     quarter, wide = extended.shape
     width, units = gate_cols.shape
-    gather_cuts, reduce_cuts = cuts(wide, 4), cuts(width, 4)
+    gather_cuts, reduce_cuts = cuts(wide, 8), cuts(width, 8)
     pieces, size = len(reduce_cuts), reduce_cuts[0][1]
     group = y_count * 2 * quarter
     vmem = pl.BlockSpec(memory_space=pltpu.VMEM)

time: 213 us -> 153 us (0.72)
  Pallas kernels: 199 us -> 139 us
    pallas_call x1, Pallas kernels: 182 us -> 122 us  [expert_rows(): pl.pallas_call(functools.partial(expert_kernel, z_count, y_count, gather_...]
where the time goes in v3:
time: 153 us; the launch traced here: 152 us
  Pallas kernels  139 us (91%)
  local copies, waits for them, and re-layouts  13.5 us (9%)
    pallas_call x1, Pallas kernels, expert_rows(): pl.pallas_call(functools.partial(expert_kernel, z_count, y_count, gather_...  122 us
    pallas_call x1, Pallas kernels, mix_rows(): pl.pallas_call(functools.partial(mix_kernel, sp_count, tp_count), out_sha...  16.6 us
    unnamed x23, local copies, waits for them, and re-layouts  12.8 us

profile of v3, /device:TPU:0, one launch (start us, length us, event | category | flops | bytes accessed | tf_op | source)
XLA Modules:
  0.0 152.4 jit_solution(11291792857288101954)
XLA Ops:
  0.0 0.7 reshape.7.ffn_gain_ref
  0.7 0.8 copy.16.weight_ref
  1.5 0.8 copy.15.routing_ref
  2.3 0.0 copy-start
  2.3 2.2 %copy-done = bf16[1024,2048]{1,0:T(8,128)(2,1)S(1)} copy-done((bf16[1024,2048]{1,0:T(8,128)(2,1)S(1)}, bf16[1024,2048]{1,0:T(8,128)(2,1)}, u32[]{:S(2)}) %copy-start) | copy-done | bytes 4194328
  4.5 0.0 copy-start.3
  4.5 0.9 copy-done.3
  5.4 0.0 copy-start.4
  5.4 0.9 copy-done.4
  6.3 0.0 copy-start.5
  6.3 0.9 copy-done.5
  7.2 0.0 copy-start.6
  7.2 0.9 copy-done.6
  8.1 0.0 copy-start.7
  8.1 0.8 copy-done.7
  9.0 0.0 copy-start.8
  9.0 0.8 copy-done.8
  9.8 0.0 copy-start.9
  9.8 0.7 copy-done.9
  10.5 16.6 %mix_rows.1 = (bf16[64,2048]{1,0:T(8,128)(2,1)S(1)}, bf16[64,2176]{1,0:T(8,128)(2,1)S(1)}) custom-call(bf16[256,128]{1,0:T(8,128)(2,1)S(1)} %copy-done.7, bf16[256,128]{1,0:T(8,128)(2,1)S(1)} %copy-done.8, bf16[256,256]{1,0:T(8,128)(2,1)S(1)} %copy-done.4, bf16[256,256]{1,0:T(8,128)(2,1)S(1)} %copy-done.5, f32[256,128]{1,0:T(8,128)S(1)} %copy-done.6, ...), custom_call_target="tpu_custom_call" | custom-call | tf_op jit(solution)/shard_map/mix_rows/pallas_call | solution.py:228
  27.1 0.0 copy-start.1
  27.1 0.7 copy-done.1
  27.8 0.0 copy-start.2
  27.8 0.7 copy-done.2
  28.5 122.2 %expert_rows.1 = bf16[64,2048]{1,0:T(8,128)(2,1)} custom-call(bf16[64,2176]{1,0:T(8,128)(2,1)} %copy-done.1, bf16[64,2048]{1,0:T(8,128)(2,1)} %copy-done.2, bf16[2048,512]{1,0:T(8,128)(2,1)} %bitcast.5, bf16[2048,512]{1,0:T(8,128)(2,1)} %bitcast.6, bf16[512,2048]{1,0:T(8,128)(2,1)} %bitcast.7), custom_call_target="tpu_custom_call" | custom-call | tf_op jit(solution)/shard_map/expert_rows/pallas_call | solution.py:465
  150.8 1.7 %copy.18 = bf16[64,2048]{1,0:T(8,128)(2,1)} copy(bf16[64,2048]{1,0:T(8,128)(2,1)} %expert_rows.1) | data formatting | bytes 524288
Async XLA Ops:
  2.3 2.2 %copy-start = (bf16[1024,2048]{1,0:T(8,128)(2,1)S(1)}, bf16[1024,2048]{1,0:T(8,128)(2,1)}, u32[]{:S(2)}) copy-start(bf16[1024,2048]{1,0:T(8,128)(2,1)} %w_hbm.1) | copy-start | bytes 12582916
  4.5 0.9 copy-start.3
  5.4 0.9 copy-start.4
  6.3 0.9 copy-start.5
  7.2 0.9 copy-start.6
  8.1 0.8 copy-start.7
  9.0 0.8 copy-start.8
  9.8 0.7 copy-start.9
  27.1 0.7 copy-start.1
  27.8 0.7 copy-start.2
